TPU v7x, 32 devices: a whole 2x2x4 slice. The times are simulated.
32 devices in a mesh: fs: 8 (over z, core), tp: 4 (over y, x).
Axes of the slice: x: 2, y: 2, z: 4, core: 2. Of those that a mesh axis runs over, the one named last changes fastest.
Arguments:
- attn_out: bfloat16 [12288, 2048], P('fs', 'tp'), may hold values from -6 to 6
- out_cot: bfloat16 [12288, 4096], P('fs', 'tp'), may hold values from -6 to 6
- latent: bfloat16 [12288, 1024], P('fs', 'tp'), may hold values from -6 to 6
- value_cot: bfloat16 [12288, 2048], P('fs', 'tp'), may hold values from -6 to 6
- out_weight: float32 [2048, 4096], P('fs', 'tp'), may hold values from -0.125 to 0.125
- value_up_matrix: float32 [1024, 2048], P('fs', 'tp'), may hold values from -0.1875 to 0.1875
- out_basis: bfloat16 [2048, 256], P('fs'), as said below
- value_basis: bfloat16 [1024, 256], P('fs'), as said below
- out_mean: float32 [256, 4096], P(None, 'tp'), may hold values from -2660.43 to 2660.43
- out_square: float32 [256, 4096], P(None, 'tp'), may hold values from 12288 to 2457600, as said below
- value_mean: float32 [256, 2048], P(None, 'tp'), may hold values from -2660.43 to 2660.43
- value_square: float32 [256, 2048], P(None, 'tp'), may hold values from 12288 to 2457600, as said below
Outputs:
- out_step: float32 [2048, 4096], P('fs', 'tp')
- out_new: float32 [2048, 4096], P('fs', 'tp')
- out_copy: bfloat16 [2048, 4096], P(None, 'tp')
- out_mean_new: float32 [256, 4096], P(None, 'tp')
- out_square_new: float32 [256, 4096], P(None, 'tp')
- value_step: float32 [1024, 2048], P('fs', 'tp')
- value_new: float32 [1024, 2048], P('fs', 'tp')
- value_copy: bfloat16 [1024, 2048], P(None, 'tp')
- value_mean_new: float32 [256, 2048], P(None, 'tp')
- value_square_new: float32 [256, 2048], P(None, 'tp')
Inputs may be any that keep to these rules, and one draw needn't show every extreme that they name: `out_basis`: factors of full rank, rows of differing scales. `value_basis`: factors of full rank, rows of differing scales. `out_square`: Positive. `value_square`: Positive.
All inputs are finite; a program needn't handle non-finite values.
Results may differ from a plain program's by a relative error of at most 0.012.
Values may be sent and summed in bfloat16 or wider, within the bound.
A program may use at most 64 MiB of HBM per device.

v0:
```python
import jax
import jax.numpy as jnp
from jax import lax
from jax.sharding import PartitionSpec as P

LEARN_RATE = 0.01
MEAN_DECAY = 0.8
BETA_SQUARE = 0.9
EPS_RMS = 1e-06


def moments(proj, mean_in, square_in):
    mean_new = MEAN_DECAY * mean_in + (1.0 - MEAN_DECAY) * proj
    square_new = BETA_SQUARE * square_in + (1.0 - BETA_SQUARE) * proj * proj
    return (mean_new, square_new, mean_new / jnp.sqrt(square_new))


def split_product(lifted, cotangent):
    upper = lifted.astype(jnp.bfloat16)
    lower = (lifted - upper.astype(jnp.float32)).astype(jnp.bfloat16)
    first = jnp.dot(upper.T, cotangent, preferred_element_type=jnp.float32)
    return first + jnp.dot(lower.T, cotangent, preferred_element_type=jnp.float32)


def per_device(
    attn_out,
    out_cot,
    latent,
    value_cot,
    out_weight,
    value_up_matrix,
    out_basis,
    value_basis,
    out_mean,
    out_square,
    value_mean,
    value_square,
):
    width_out = out_cot.shape[1]
    head_cols = value_cot.shape[1]
    rows_out = out_basis.shape[0]
    rows_value = value_basis.shape[0]
    all_heads, all_latent = (
        lax.all_gather(attn_out, "tp", axis=1, tiled=True),
        lax.all_gather(latent, "tp", axis=1, tiled=True),
    )
    whole_o, whole_v = (
        lax.all_gather(out_basis, "fs", axis=0, tiled=True),
        lax.all_gather(value_basis, "fs", axis=0, tiled=True),
    )
    lifted_o = jnp.dot(all_heads, whole_o, preferred_element_type=jnp.float32)
    part_o = split_product(lifted_o, out_cot)
    lifted_v = jnp.dot(all_latent, whole_v, preferred_element_type=jnp.float32)
    part_v = split_product(lifted_v, value_cot)
    count_o = rows_out * lax.axis_size("fs") * width_out * lax.axis_size("tp")
    count_v = rows_value * lax.axis_size("fs") * head_cols * lax.axis_size("tp")
    proj_o, proj_v = (
        lax.psum(part_o.astype(jnp.bfloat16), "fs").astype(jnp.float32),
        lax.psum(part_v.astype(jnp.bfloat16), "fs").astype(jnp.float32),
    )
    mean_o, square_o, direction_o = moments(proj_o, out_mean, out_square)
    mean_v, square_v, direction_v = moments(proj_v, value_mean, value_square)
    update_o = jnp.dot(out_basis.astype(jnp.float32), direction_o, precision=lax.Precision.HIGHEST)
    update_v = jnp.dot(
        value_basis.astype(jnp.float32), direction_v, precision=lax.Precision.HIGHEST
    )
    total_o, total_v = lax.psum(
        (jnp.sum(update_o * update_o), jnp.sum(update_v * update_v)), ("fs", "tp")
    )
    step_o = LEARN_RATE * update_o * lax.rsqrt(total_o / count_o + EPS_RMS)
    step_v = LEARN_RATE * update_v * lax.rsqrt(total_v / count_v + EPS_RMS)
    new_o = out_weight - step_o
    new_v = value_up_matrix - step_v
    copy_o, copy_v = (
        lax.all_gather(new_o.astype(jnp.bfloat16), "fs", axis=0, tiled=True),
        lax.all_gather(new_v.astype(jnp.bfloat16), "fs", axis=0, tiled=True),
    )
    return (step_o, new_o, copy_o, mean_o, square_o, step_v, new_v, copy_v, mean_v, square_v)


def solution(mesh):
    placed = (
        P("fs", "tp"),
        P("fs", "tp"),
        P("fs", "tp"),
        P("fs", "tp"),
        P("fs", "tp"),
        P("fs", "tp"),
        P("fs", None),
        P("fs", None),
        P(None, "tp"),
        P(None, "tp"),
        P(None, "tp"),
        P(None, "tp"),
    )
    return jax.shard_map(
        per_device,
        mesh=mesh,
        in_specs=placed,
        out_specs=(
            P("fs", "tp"),
            P("fs", "tp"),
            P(None, "tp"),
            P(None, "tp"),
            P(None, "tp"),
            P("fs", "tp"),
            P("fs", "tp"),
            P(None, "tp"),
            P(None, "tp"),
            P(None, "tp"),
        ),
        check_vma=False,
    )
```

profile of v0, /device:TPU:0, one launch (start us, length us, event | category | flops | bytes accessed | tf_op | source)
XLA Modules:
  0.0 352.1 jit_solution(6366198598271107823)
XLA Ops:
  7.2 0.7 all-gather.12.cloned.1.call-update
  8.0 0.7 all-gather.8.cloned.1.call-update
  8.7 0.7 all-gather.6.cloned.1.call-update
  9.5 17.5 %all_gather.22 = bf16[1024,256]{1,0:T(8,128)(2,1)} all-gather(bf16[128,256]{1,0:T(8,128)(2,1)S(1)} %copy-done.11), channel_id=1, replica_groups=mesh['fs'=8,'tp'=4] {'fs'}, dimensions={0}, use_global_device_ids=true | all-gather | bytes 589824 | tf_op jit(solution)/shard_map/all_gather | solution.py:49
  27.0 29.3 %all-gather.12.cloned.1.call-done = bf16[1536,1024]{1,0:T(8,128)(2,1)} async-done(((bf16[1536,256]{1,0:T(8,128)(2,1)}), bf16[1536,1024]{1,0:T(8,128)(2,1)}) %all-gather.12.cloned.1.call-update) | async-done | bytes 3145744 | tf_op jit(solution)/shard_map/all_gather | solution.py:45
  56.3 3.1 fusion.21
  59.4 0.6 fusion.13
  60.0 1.3 fusion.1
  61.3 18.8 %all-gather.8.cloned.1.call-done = bf16[2048,256]{1,0:T(8,128)(2,1)} async-done(((bf16[256,256]{1,0:T(8,128)(2,1)}), bf16[2048,256]{1,0:T(8,128)(2,1)}) %all-gather.8.cloned.1.call-update) | async-done | bytes 1048592 | tf_op jit(solution)/shard_map/all_gather | solution.py:48
  80.2 71.4 %all-gather.6.cloned.1.call-done = bf16[1536,2048]{1,0:T(8,128)(2,1)} async-done(((bf16[1536,512]{1,0:T(8,128)(2,1)}), bf16[1536,2048]{1,0:T(8,128)(2,1)}) %all-gather.6.cloned.1.call-update) | async-done | bytes 6291472 | tf_op jit(solution)/shard_map/all_gather | solution.py:44
  151.5 4.9 %fusion.20 = f32[1536,256]{1,0:T(8,128)S(1)} fusion(bf16[1536,2048]{1,0:T(8,128)(2,1)} %all-gather.6.cloned.1.call-done, bf16[2048,256]{1,0:T(8,128)(2,1)} %all-gather.8.cloned.1.call-done), kind=kOutput, calls=%fused_computation.32 | convolution fusion | flops 1610612736 | bytes 8912896 | tf_op jit(solution)/shard_map/dot_general | solution.py:51
  156.5 1.0 fusion.16
  157.5 1.8 fusion
  159.4 0.8 copy.23
  160.2 57.0 %all-reduce.4.cloned.1.call-done = (bf16[256,1024]{1,0:T(8,128)(2,1)}, bf16[256,512]{1,0:T(8,128)(2,1)}) async-done(((bf16[256,1024]{1,0:T(8,128)(2,1)}, bf16[256,512]{1,0:T(8,128)(2,1)}), (bf16[256,1024]{1,0:T(8,128)(2,1)}, bf16[256,512]{1,0:T(8,128)(2,1)})) %all-reduce.4.cloned.1.call-update) | async-done | bytes 786448 | tf_op jit(solution)/shard_map/psum | solution.py:58
  217.3 2.1 fusion.3
  219.4 2.6 multiply_reduce_fusion
  222.0 0.2 fusion.8
  222.2 0.8 copy-done.4
  223.0 1.2 multiply_reduce_fusion.1
  224.2 39.5 %all-reduce = (f32[]{:T(128)}, f32[]{:T(128)}) all-reduce(f32[]{:T(128)} %get-tuple-element.34, f32[]{:T(128)} %get-tuple-element.36), channel_id=1, replica_groups=mesh['fs'=8,'tp'=4] {'fs','tp'}, use_global_device_ids=true, to_apply=%region_2.0 | all-reduce | flops 2 | bytes 16 | tf_op jit(solution)/shard_map/psum | solution.py:67
  264.4 1.8 fusion.18
  266.3 2.5 copy.22
  269.5 3.2 fusion.19
  272.8 2.6 copy.24
  275.4 2.6 copy.25
  277.9 1.8 copy.27
  279.7 0.8 copy.28
  280.6 9.7 %all-gather.14.cloned.1.call-done = bf16[1024,512]{0,1:T(8,128)(2,1)} async-done(((bf16[128,512]{0,1:T(8,128)(2,1)}), bf16[1024,512]{0,1:T(8,128)(2,1)}) %all-gather.14.cloned.1.call-update) | async-done | bytes 1048592 | tf_op jit(solution)/shard_map/all_gather | solution.py:76
  290.3 2.3 copy.29
  292.6 46.4 %all-gather.10.cloned.1.call-done = bf16[2048,1024]{0,1:T(8,128)(2,1)} async-done(((bf16[256,1024]{0,1:T(8,128)(2,1)}), bf16[2048,1024]{0,1:T(8,128)(2,1)}) %all-gather.10.cloned.1.call-update) | async-done | bytes 4194320 | tf_op jit(solution)/shard_map/all_gather | solution.py:75
  338.9 6.4 %copy.26 = bf16[2048,1024]{1,0:T(8,128)(2,1)} copy(bf16[2048,1024]{0,1:T(8,128)(2,1)} %all-gather.10.cloned.1.call-done) | data formatting | bytes 8388608
  (34 shorter events, 0.4 us)
Async XLA Ops:
  7.2 149.3 %copy-start = (bf16[1536,1024]{1,0:T(8,128)(2,1)S(1)}, bf16[1536,1024]{1,0:T(8,128)(2,1)}, u32[]{:S(2)}) copy-start(bf16[1536,1024]{1,0:T(8,128)(2,1)} %param.13) | copy-start | bytes 9437188
  7.2 2.3 copy-start.11
  7.2 49.1 %all-gather.12.cloned.1.call-start = ((), (), s32[]{:S(2)}) async-start(), calls=%async_computation.3 | async-start | bytes 3932160 | tf_op jit(solution)/shard_map/all_gather | solution.py:45
  7.9 72.2 %all-gather.8.cloned.1.call-start = ((), (), s32[]{:S(2)}) async-start(), calls=%async_computation.1 | async-start | bytes 1179648 | tf_op jit(solution)/shard_map/all_gather | solution.py:48
  8.7 142.8 %all-gather.6.cloned.1.call-start = ((), (), s32[]{:S(2)}) async-start(), calls=%async_computation | async-start | bytes 7864320 | tf_op jit(solution)/shard_map/all_gather | solution.py:44
  9.4 207.9 %all-reduce.4.cloned.1.call-start = ((), (), s32[]{:S(2)}) async-start(), calls=%async_computation.5 | async-start | bytes 1572864 | tf_op jit(solution)/shard_map/psum | solution.py:58
  56.3 3.1 copy-start.1
  157.5 1.9 copy-start.12
  159.3 130.9 %all-gather.14.cloned.1.call-start = ((), (), s32[]{:S(2)}) async-start(), calls=%async_computation.4 | async-start | bytes 1179648 | tf_op jit(solution)/shard_map/all_gather | solution.py:76
  217.3 2.1 copy-start.7
  219.3 2.7 copy-start.2
  219.4 2.7 copy-start.3
  219.4 2.6 copy-start.8
  219.4 2.6 copy-start.9
  219.4 2.6 copy-start.10
  222.2 0.8 copy-start.4
  222.2 2.0 copy-start.5
  266.3 72.6 %all-gather.10.cloned.1.call-start = ((), (), s32[]{:S(2)}) async-start(), calls=%async_computation.2 | async-start | bytes 4718592 | tf_op jit(solution)/shard_map/all_gather | solution.py:75
  275.4 4.4 %copy-start.6 = (f32[128,512]{0,1:T(8,128)S(1)}, f32[128,512]{0,1:T(8,128)}, u32[]{:S(2)}) copy-start(f32[128,512]{0,1:T(8,128)} %get-tuple-element.25) | copy-start | bytes 786436
Sparse Core Ops, SparseCore 0:
  9.8 46.4 all-gather.11
  57.9 22.2 all-gather.7
  82.0 69.4 all-gather.5
  159.5 57.7 all-reduce.3
  266.4 23.8 all-gather.13
  292.3 46.5 all-gather.9
where the time goes:
time: 353 us; the launch traced here: 352 us
  waiting for transfers between devices  235 us (67%)
  blocking collectives  57 us (16%)
  local copies, waits for them, and re-layouts  20.6 us (6%)
  matrix products  16.6 us (5%)
  between operations  15.7 us (4%)
  other arithmetic  7.29 us (2%)
    all_gather x1, waiting for transfers between devices, per_device(): lax.all_gather(attn_out, 'tp', axis=1, tiled=True)  71.4 us
    psum x1, waiting for transfers between devices, per_device(): lax.psum(part_o.astype(jnp.bfloat16), 'fs').astype(jnp.float32)  57 us
    all_gather x1, waiting for transfers between devices, per_device(): lax.all_gather(new_o.astype(jnp.bfloat16), 'fs', axis=0, tiled=True)  46.4 us
    psum x1, blocking collectives, per_device(): lax.psum((jnp.sum(update_o * update_o), jnp.sum(update_v * update_v)), ('...  39.5 us
    all_gather x1, waiting for transfers between devices, per_device(): lax.all_gather(latent, 'tp', axis=1, tiled=True)  29.3 us
    unnamed x34, local copies, waits for them, and re-layouts  20.6 us
    all_gather x1, waiting for transfers between devices, per_device(): lax.all_gather(out_basis, 'fs', axis=0, tiled=True)  18.8 us
    all_gather x1, blocking collectives, per_device(): lax.all_gather(value_basis, 'fs', axis=0, tiled=True)  17.5 us
  transfers between devices with their start and end apart: 6, of which 6 were waited for; matrix products, arithmetic and copies ran while one was open for 6% of the time, Pallas kernels for 0%

commit v1 on v0

v1 whole, which is shorter than its diff:
```python
import functools

import jax
import jax.numpy as jnp
from jax import lax
from jax.experimental import pallas as pl
from jax.experimental.pallas import tpu as pltpu
from jax.sharding import PartitionSpec as P

LEARN_RATE = 0.01
MEAN_DECAY = 0.8
BETA_SQUARE = 0.9
EPS_RMS = 1e-06
MESH = pl.DeviceIdType.MESH
F32, BF16 = jnp.float32, jnp.bfloat16


def moments(proj, mean_in, square_in):
    mean_new = MEAN_DECAY * mean_in + (1.0 - MEAN_DECAY) * proj
    square_new = BETA_SQUARE * square_in + (1.0 - BETA_SQUARE) * proj * proj
    return (mean_new, square_new, mean_new / jnp.sqrt(square_new))


def rcopy(src, dst, send, recv, fs, tp):
    return pltpu.make_async_remote_copy(
        src_ref=src, dst_ref=dst, send_sem=send, recv_sem=recv,
        device_id=(fs, tp), device_id_type=MESH,
    )


class LineGather:
    def __init__(self, own, buf, up, dn, d2, rz, rd, nz, f, t):
        self.own, self.buf, self.nz, self.t, self.f = own, buf, nz, t, f
        self.up, self.dn, self.d2, self.rz, self.rd = up, dn, d2, rz, rd
        self.z, self.c = lax.div(f, 2), lax.rem(f, 2)
        self.partner = f + 1 - 2 * self.c

    def copy(self, kind, zb, src=None):
        block = self.buf.at[zb * 2 + self.c]
        src = block if src is None else src
        if kind == "up":
            return rcopy(src, block, self.up.at[zb], self.rz.at[zb], self.f + 2, self.t)
        if kind == "dn":
            return rcopy(src, block, self.dn.at[zb], self.rz.at[zb], self.f - 2, self.t)
        return rcopy(src, block, self.d2.at[zb], self.rd.at[zb], self.partner, self.t)

    def spread(self, zb, src, up, dn):
        if up:
            @pl.when(self.z < self.nz - 1)
            def _():
                self.copy("up", zb, src).start()
        if dn:
            @pl.when(self.z > 0)
            def _():
                self.copy("dn", zb, src).start()
        self.copy("d2", zb, src).start()

    def begin(self):
        self.spread(self.z, self.own, True, True)

    def step(self, s):
        @pl.when(self.z >= s)
        def _():
            zb = self.z - s
            rcopy(self.buf.at[zb * 2 + self.c], self.buf.at[zb * 2 + self.c], self.up.at[zb],
                  self.rz.at[zb], self.partner, self.t).wait_recv()
            self.spread(zb, None, True, False)

        @pl.when(self.z + s <= self.nz - 1)
        def _():
            zb = self.z + s
            rcopy(self.buf.at[zb * 2 + self.c], self.buf.at[zb * 2 + self.c], self.dn.at[zb],
                  self.rz.at[zb], self.partner, self.t).wait_recv()
            self.spread(zb, None, False, True)

    def arrive(self):
        for zb in range(self.nz):
            block = self.buf.at[zb * 2 + 1 - self.c]
            rcopy(block, block, self.d2.at[zb], self.rd.at[zb], self.partner, self.t).wait_recv()

    def finish(self):
        for zb in range(self.nz):
            self.copy("d2", zb).wait_send()

            @pl.when((self.z >= zb) & (self.z < self.nz - 1))
            def _():
                self.copy("up", zb).wait_send()

            @pl.when((self.z <= zb) & (self.z > 0))
            def _():
                self.copy("dn", zb).wait_send()


def exchange(nf, nt, ro, rv,
             attn, ocot, lat, vcot, w_o, w_v, basis, mean_o, sq_o, mean_v, sq_v,
             proj_out, wg_o, wg_v, bg_out, totals,
             bg, lift, rsb, lifted, part, psend, pbuf, zsend, zbuf, tot, tsend, tbuf, dirs,
             lsem, bsem, wsem, rs_s, rs_r, ag_s, ag_r, p_sem, z_s, z_r,
             g_s, g_r, gd_s, gd_r, t_s, t_r):
    nz = nf // 2
    f, t = lax.axis_index("fs"), lax.axis_index("tp")
    z, c = lax.div(f, 2), lax.rem(f, 2)
    partner = f + 1 - 2 * c
    tokens, wo = ocot.shape
    rank = basis.shape[1]
    tc, seg, per = tokens // nt, rank // nf, nf // nt
    peers_t = [lax.rem(t + s, nt) for s in range(1, nt)]
    peers_z = [lax.rem(z + s, nz) for s in range(1, nz)]

    barrier = pltpu.get_barrier_semaphore()
    pl.semaphore_signal(barrier, inc=1, device_id=(partner, t), device_id_type=MESH)
    for pz in peers_z:
        pl.semaphore_signal(barrier, inc=1, device_id=(pz * 2 + c, t), device_id_type=MESH)
    for pt in peers_t:
        pl.semaphore_signal(barrier, inc=1, device_id=(f, pt), device_id_type=MESH)
    pl.semaphore_wait(barrier, 1 + len(peers_z) + len(peers_t))

    gb = LineGather(basis, bg, *[bsem.at[k] for k in range(5)], nz, f, t)
    gw = [LineGather(own, buf, *[wsem.at[i, k] for k in range(5)], nz, f, t)
          for i, (own, buf) in enumerate(((w_o, wg_o), (w_v, wg_v)))]
    gb.begin()
    bg[f] = basis[...]
    mine = [pltpu.make_async_copy(own, buf.at[f], lsem.at[i])
            for i, (own, buf) in enumerate(((w_o, wg_o), (w_v, wg_v)))]
    for m in mine:
        m.start()
    for s in range(1, nz):
        gb.step(s)
    for g in gw:
        g.begin()
    gb.arrive()

    rows = bg[pl.ds(t * per, per)]
    b_o = rows[:, :ro, :].reshape(per * ro, rank)
    b_v = rows[:, ro:, :].reshape(per * rv, rank)
    waiting = None
    for pt in peers_t + [t]:
        at = pl.ds(pl.multiple_of(pt * tc, tc), tc)
        lift[pt, :, :rank] = jnp.dot(attn[at, :], b_o, preferred_element_type=F32).astype(BF16)
        lift[pt, :, rank:] = jnp.dot(lat[at, :], b_v, preferred_element_type=F32).astype(BF16)
        if waiting is not None:
            waiting.start()
        waiting = None
        if pt is not t:
            waiting = rcopy(lift.at[pt], rsb.at[t], rs_s.at[pt], rs_r.at[t], f, pt)

    third = (nz - 1 + 2) // 3
    steps = list(range(1, nz))
    for s in steps[:third]:
        for g in gw:
            g.step(s)

    total = lift[t].astype(F32)
    for pt in peers_t:
        rcopy(lift.at[pt], rsb.at[pt], rs_s.at[pt], rs_r.at[pt], f, pt).wait_recv()
        total = total + rsb[pt].astype(F32)
    lifted[t] = total.astype(BF16)
    for pt in peers_t:
        rcopy(lifted.at[t], lifted.at[t], ag_s.at[pt], ag_r.at[t], f, pt).start()

    def contract(pt, first):
        at = pl.ds(pl.multiple_of(pt * tc, tc), tc)
        dims = (((0,), (0,)), ((), ()))
        o = lax.dot_general(lifted[pt, :, :rank], ocot[at, :], dims, preferred_element_type=F32)
        v = lax.dot_general(lifted[pt, :, rank:], vcot[at, :], dims, preferred_element_type=F32)
        if first:
            part[:, :wo] = o
            part[:, wo:] = v
        else:
            part[:, :wo] += o
            part[:, wo:] += v

    contract(t, True)
    for s in steps[third:2 * third]:
        for g in gw:
            g.step(s)
    for pt in peers_t:
        rcopy(lifted.at[pt], lifted.at[pt], ag_s.at[pt], ag_r.at[pt], f, pt).wait_recv()
        contract(pt, False)

    def piece(core, zz):
        return part[pl.ds(pl.multiple_of((core * nz + zz) * seg, seg), seg), :]

    for zz in range(nz):
        psend[zz] = piece(1 - c, zz).astype(BF16)
    pair = rcopy(psend, pbuf, p_sem.at[0], p_sem.at[1], partner, t)
    pair.start()
    pair.wait_recv()
    for pz in peers_z:
        zsend[pz] = (piece(c, pz) + pbuf[pz].astype(F32)).astype(BF16)
    for pz in peers_z:
        rcopy(zsend.at[pz], zbuf.at[z], z_s.at[pz], z_r.at[z], pz * 2 + c, t).start()
    acc = piece(c, z) + pbuf[z].astype(F32)
    for pz in peers_z:
        rcopy(zsend.at[pz], zbuf.at[pz], z_s.at[pz], z_r.at[pz], pz * 2 + c, t).wait_recv()
        acc = acc + zbuf[pz].astype(F32)
    me = c * nz + z
    tot[me] = acc.astype(BF16)
    for pz in peers_z:
        rcopy(tot.at[me], tot.at[me], g_s.at[pz], g_r.at[z], pz * 2 + c, t).start()
    rcopy(tot.at[me], tot.at[me], gd_s.at[z], gd_r.at[z], partner, t).start()
    for s in steps[2 * third:]:
        for g in gw:
            g.step(s)
    for pz in peers_z:
        got = tot.at[c * nz + pz]
        rcopy(got, got, g_s.at[pz], g_r.at[pz], pz * 2 + c, t).wait_recv()
        rcopy(got, got, gd_s.at[pz], gd_r.at[pz], partner, t).start()
    for zz in range(nz):
        got = tot.at[(1 - c) * nz + zz]
        rcopy(got, got, gd_s.at[zz], gd_r.at[zz], partner, t).wait_recv()

    proj = tot[...].astype(F32).reshape(rank, part.shape[1])
    part[...] = proj
    dirs[:, :wo] = moments(part[:, :wo], mean_o[...], sq_o[...])[2].astype(BF16)
    dirs[:, wo:] = moments(part[:, wo:], mean_v[...], sq_v[...])[2].astype(BF16)
    proj_out[...] = part[...]
    bg_out[...] = bg[...]

    def squares(g, sums):
        u_o = jnp.dot(bg[g, :ro, :], dirs[:, :wo], preferred_element_type=F32)
        u_v = jnp.dot(bg[g, ro:, :], dirs[:, wo:], preferred_element_type=F32)
        return (sums[0] + jnp.sum(u_o * u_o, axis=0, keepdims=True),
                sums[1] + jnp.sum(u_v * u_v, axis=0, keepdims=True))

    sums = lax.fori_loop(0, nf, squares, (jnp.zeros((1, wo), F32),
                                          jnp.zeros((1, part.shape[1] - wo), F32)))
    for k in range(2):
        tile = jnp.zeros((8, 128), F32) + jnp.sum(sums[k], axis=1, keepdims=True)
        tsend[k] = tile
        tbuf[t, k] = tile
    for pt in peers_t:
        rcopy(tsend, tbuf.at[t], t_s.at[pt], t_r.at[t], f, pt).start()
    for m in mine:
        m.wait()
    for g in gw:
        g.arrive()
    for pt in peers_t:
        rcopy(tsend, tbuf.at[pt], t_s.at[pt], t_r.at[pt], f, pt).wait_recv()
    summed = tbuf[0]
    for k in range(1, nt):
        summed = summed + tbuf[k]
    totals[...] = summed

    gb.finish()
    for g in gw:
        g.finish()
    pair.wait_send()
    for pt in peers_t:
        rcopy(lift.at[pt], rsb.at[t], rs_s.at[pt], rs_r.at[t], f, pt).wait_send()
        rcopy(lifted.at[t], lifted.at[t], ag_s.at[pt], ag_r.at[t], f, pt).wait_send()
        rcopy(tsend, tbuf.at[t], t_s.at[pt], t_r.at[t], f, pt).wait_send()
    for pz in peers_z:
        rcopy(zsend.at[pz], zbuf.at[z], z_s.at[pz], z_r.at[z], pz * 2 + c, t).wait_send()
        rcopy(tot.at[me], tot.at[me], g_s.at[pz], g_r.at[z], pz * 2 + c, t).wait_send()
    for zz in range(nz):
        got = tot.at[c * nz + zz]
        rcopy(got, got, gd_s.at[zz], gd_r.at[zz], partner, t).wait_send()


def gather_and_reduce(nf, nt, attn, ocot, lat, vcot, w_o, w_v, b_o, b_v, mean_o, sq_o, mean_v, sq_v):
    ro, rv, rank = b_o.shape[0], b_v.shape[0], b_o.shape[1]
    nz, wo, wv, tokens = nf // 2, ocot.shape[1], vcot.shape[1], ocot.shape[0]
    width, tc, seg = wo + wv, tokens // nt, rank // nf
    basis = jnp.concatenate((b_o, b_v), axis=0)
    vmem, hbm, dma = pl.BlockSpec(memory_space=pltpu.VMEM), pl.BlockSpec(memory_space=pl.ANY), pltpu.SemaphoreType.DMA
    return pl.pallas_call(
        functools.partial(exchange, nf, nt, ro, rv),
        out_shape=(
            jax.ShapeDtypeStruct((rank, width), F32),
            jax.ShapeDtypeStruct((nf, ro, wo), BF16),
            jax.ShapeDtypeStruct((nf, rv, wv), BF16),
            jax.ShapeDtypeStruct((nf, ro + rv, rank), BF16),
            jax.ShapeDtypeStruct((2, 8, 128), F32),
        ),
        in_specs=[vmem] * 11,
        out_specs=(vmem, hbm, hbm, vmem, vmem),
        scratch_shapes=[
            pltpu.VMEM((nf, ro + rv, rank), BF16),
            pltpu.VMEM((nt, tc, 2 * rank), BF16),
            pltpu.VMEM((nt, tc, 2 * rank), BF16),
            pltpu.VMEM((nt, tc, 2 * rank), BF16),
            pltpu.VMEM((rank, width), F32),
            pltpu.VMEM((nz, seg, width), BF16),
            pltpu.VMEM((nz, seg, width), BF16),
            pltpu.VMEM((nz, seg, width), BF16),
            pltpu.VMEM((nz, seg, width), BF16),
            pltpu.VMEM((nf, seg, width), BF16),
            pltpu.VMEM((2, 8, 128), F32),
            pltpu.VMEM((nt, 2, 8, 128), F32),
            pltpu.VMEM((rank, width), BF16),
            dma((2,)), dma((5, nz)), dma((2, 5, nz)),
            dma((nt,)), dma((nt,)), dma((nt,)), dma((nt,)), dma((2,)),
            dma((nz,)), dma((nz,)), dma((nz,)), dma((nz,)), dma((nz,)), dma((nz,)),
            dma((nt,)), dma((nt,)),
        ],
        compiler_params=pltpu.CompilerParams(
            collective_id=0, has_side_effects=True, vmem_limit_bytes=56 * 1024 * 1024
        ),
        name="exchange",
    )(attn, ocot, lat, vcot, w_o.astype(BF16), w_v.astype(BF16), basis, mean_o, sq_o, mean_v, sq_v)


def per_device(nf, nt, attn_out, out_cot, latent, value_cot, out_weight, value_up_matrix,
               out_basis, value_basis, out_mean, out_square, value_mean, value_square):
    proj, wg_o, wg_v, bg, totals = gather_and_reduce(
        nf, nt, attn_out, out_cot, latent, value_cot, out_weight, value_up_matrix,
        out_basis, value_basis, out_mean, out_square, value_mean, value_square)
    ro, rv, wo = out_basis.shape[0], value_basis.shape[0], out_cot.shape[1]

    def finish(proj, mean_in, square_in, total, weight, gathered, whole, basis):
        rows = whole.shape[0] * whole.shape[1]
        mean, square, direction = moments(proj, mean_in, square_in)
        narrow = direction.astype(BF16)
        count = rows * weight.shape[1] * nt
        scale = LEARN_RATE * lax.rsqrt(total / count + EPS_RMS)
        step = scale * jnp.dot(basis, narrow, preferred_element_type=F32)
        every = jnp.dot(whole.reshape(rows, -1), narrow, preferred_element_type=F32)
        copy = (gathered.reshape(rows, -1).astype(F32) - scale * every).astype(BF16)
        return (step, weight - step, copy, mean, square)

    first = finish(proj[:, :wo], out_mean, out_square, totals[0, 0, 0], out_weight, wg_o, bg[:, :ro], out_basis)
    second = finish(proj[:, wo:], value_mean, value_square, totals[1, 0, 0], value_up_matrix, wg_v, bg[:, ro:], value_basis)
    return first + second


def solution(mesh):
    both, rows, cols = P("fs", "tp"), P("fs", None), P(None, "tp")
    return jax.shard_map(
        functools.partial(per_device, mesh.shape["fs"], mesh.shape["tp"]),
        mesh=mesh,
        in_specs=(both,) * 6 + (rows,) * 2 + (cols,) * 4,
        out_specs=(both, both, cols, cols, cols) * 2,
        check_vma=False,
    )
```

time: 353 us -> 122 us (0.35)
  waiting for transfers between devices: 235 us -> 0 us
  Pallas kernels: 0 us -> 97.9 us
  blocking collectives: 57 us -> 0 us
  local copies, waits for them, and re-layouts: 20.6 us -> 6.39 us
  between operations: 15.7 us -> 2.68 us
  matrix products: 16.6 us -> 6.36 us
    all_gather x5 -> x0, waiting for transfers between devices: 176 us -> none  [the longest x1 71.4 us: per_device(): lax.all_gather(attn_out, 'tp', axis=1, tiled=True)]
    pallas_call x0 -> x1, Pallas kernels: none -> 97.9 us  [gather_and_reduce(): pl.pallas_call(functools.partial(exchange, nf, nt, ro, rv), out_shape=(ja...]
    psum x1 -> x0, waiting for transfers between devices: 57 us -> none  [per_device(): lax.psum(part_o.astype(jnp.bfloat16), 'fs').astype(jnp.float32)]
    psum x1 -> x0, blocking collectives: 39.5 us -> none  [per_device(): lax.psum((jnp.sum(update_o * update_o), jnp.sum(update_v * update_v)), ('...]
    all_gather x1 -> x0, blocking collectives: 17.5 us -> none  [per_device(): lax.all_gather(value_basis, 'fs', axis=0, tiled=True)]
    unnamed x34 -> x32, local copies, waits for them, and re-layouts: 20.6 us -> 4.93 us
    dot_general x8 -> x4, matrix products: 16.6 us -> 6.36 us  [the longest x2 4.68 us: finish(): every = jnp.dot(whole.reshape(rows, -1), narrow, preferred_element_type=F32)]
  transfers between devices with their start and end apart: 6 -> 0, of which waited for: 6 -> 0; matrix products, arithmetic and copies ran while one was open for 6% -> 0% of each run, Pallas kernels for 0% -> 0%
where the time goes in v1:
time: 122 us
  Pallas kernels  97.9 us (80%)
  other arithmetic  8.53 us (7%)
  local copies, waits for them, and re-layouts  6.39 us (5%)
  matrix products  6.36 us (5%)
  between operations  2.68 us (2%)
    pallas_call x1, Pallas kernels, gather_and_reduce(): pl.pallas_call(functools.partial(exchange, nf, nt, ro, rv), out_shape=(ja...  97.9 us
    unnamed x32, local copies, waits for them, and re-layouts  4.93 us
    dot_general x2, matrix products, finish(): every = jnp.dot(whole.reshape(rows, -1), narrow, preferred_element_type=F32)  4.68 us
    convert_element_type x2, other arithmetic, finish(): narrow = direction.astype(BF16)  4.08 us

profile of v1, /device:TPU:0, one launch (start us, length us, event | category | flops | bytes accessed | tf_op | source)
XLA Modules:
  0.0 121.9 jit_solution(13782243589825683334)
XLA Ops:
  0.6 0.0 copy-start.9
  0.7 2.1 %convert_element_type.30.w_o = bf16[256,1024]{1,0:T(8,128)(2,1)} convert(f32[256,1024]{1,0:T(8,128)} %param.16) | non-fusion elementwise | flops 262144 | bytes 1572864 | tf_op jit(solution)/shard_map/convert_element_type | solution.py:301
  2.8 1.6 %pad_maximum_fusion.basis = bf16[384,256]{1,0:T(8,128)(2,1)} fusion(bf16[128,256]{1,0:T(8,128)(2,1)} %param.19, bf16[256,256]{1,0:T(8,128)(2,1)} %param.18), kind=kLoop, calls=%fused_computation.16 | loop fusion | flops 393216 | bytes 393216 | tf_op jit(solution)/shard_map/concatenate | solution.py:265
  4.4 0.0 copy-done.9
  4.4 0.7 convert_element_type.31.w_v
  5.1 97.9 %exchange.1 = (f32[256,1536]{1,0:T(8,128)}, bf16[8,256,1024]{2,1,0:T(8,128)(2,1)}, bf16[8,128,512]{2,1,0:T(8,128)(2,1)}, bf16[8,384,256]{2,1,0:T(8,128)(2,1)}, f32[2,8,128]{2,1,0:T(8,128)}) custom-call(bf16[1536,512]{1,0:T(8,128)(2,1)} %attn.1, bf16[1536,1024]{1,0:T(8,128)(2,1)} %ocot.1, bf16[1536,256]{1,0:T(8,128)(2,1)} %lat.1, bf16[1536,512]{1,0:T(8,128)(2,1)} %vcot.1, ...), custom_call_target="tpu_custom_call" | custom-call | tf_op jit(solution)/shard_map/exchange/pallas_call | solution.py:267
  103.1 0.0 copy-start.6
  103.1 0.0 copy-start.8
  103.1 0.0 copy-done.4
  103.1 0.0 copy-done.5
  103.1 2.4 %multiply_convert_fusion.1 = (bf16[256,512]{1,0:T(8,128)(2,1)S(1)}, f32[256,512]{1,0:T(8,128)}, f32[256,512]{1,0:T(8,128)}) fusion(f32[256,1536]{1,0:T(8,128)} %get-tuple-element.16, f32[256,512]{1,0:T(8,128)S(1)} %copy-done.5, f32[256,512]{1,0:T(8,128)S(1)} %copy-done.4), kind=kLoop, calls=%fused_computation.14 | loop fusion | flops 1179648 | bytes 2883584 | tf_op jit(solution)/shard_map/convert_element_type | solution.py:314
  105.5 1.3 %fusion.8 = (f32[1,1,1]{2,1,0:T(1,128)}, f32[1,1,1]{2,1,0:T(1,128)}) fusion(f32[2,8,128]{2,1,0:T(8,128)} %get-tuple-element.15), kind=kLoop, calls=%fused_computation.17 | loop fusion | bytes 16 | tf_op jit(solution)/shard_map/slice | solution.py:323
  107.5 0.0 copy-done.6
  107.6 0.0 copy-done.8
  107.6 1.4 %fusion.1 = bf16[1024,512]{1,0:T(8,128)(2,1)} fusion(bf16[1024,512]{1,0:T(8,128)(2,1)S(1)} %bitcast.21, bf16[1024,256]{1,0:T(8,128)(2,1)S(1)} %bitcast.20, bf16[256,512]{1,0:T(8,128)(2,1)S(1)} %get-tuple-element.30, f32[]{:T(128)} %bitcast.4), kind=kOutput, calls=%fused_computation.3 | convolution fusion | flops 270532608 | bytes 2883588 | tf_op jit(solution)/shard_map/dot_general | solution.py:318
  109.0 0.0 copy-done.1
  109.0 0.0 copy-done.2
  109.0 0.0 copy-done.7
  109.0 1.7 %multiply_convert_fusion = (bf16[256,1024]{1,0:T(8,128)(2,1)S(1)}, f32[256,1024]{1,0:T(8,128)}, f32[256,1024]{1,0:T(8,128)}) fusion(f32[256,1536]{1,0:T(8,128)S(1)} %copy-done.7, f32[256,1024]{1,0:T(8,128)S(1)} %copy-done.2, f32[256,1024]{1,0:T(8,128)S(1)} %copy-done.1), kind=kLoop, calls=%fused_computation.10 | loop fusion | flops 2359296 | bytes 5767168 | tf_op jit(solution)/shard_map/convert_element_type | solution.py:314
  111.9 0.1 slice.20
  112.0 0.1 copy-done.12
  112.1 3.3 %fusion = bf16[2048,1024]{1,0:T(8,128)(2,1)} fusion(bf16[2048,1024]{1,0:T(8,128)(2,1)S(1)} %bitcast.23, bf16[2048,256]{1,0:T(8,128)(2,1)S(1)} %bitcast.22, bf16[256,1024]{1,0:T(8,128)(2,1)S(1)} %get-tuple-element.33, f32[]{:T(128)} %bitcast), kind=kOutput, calls=%fused_computation.1 | convolution fusion | flops 1082130432 | bytes 9961476 | tf_op jit(solution)/shard_map/dot_general | solution.py:318
  115.4 0.1 copy.23
  115.6 0.0 copy-start.10
  115.6 0.3 fusion.10
  115.8 0.8 copy.26
  116.7 0.8 copy.27
  117.5 0.0 copy-done
  117.5 0.3 copy.22
  117.9 1.4 %fusion.9 = (f32[256,1024]{0,1:T(8,128)S(1)}, f32[256,1024]{0,1:T(8,128)S(1)}) fusion(f32[256,1024]{0,1:T(8,128)S(1)} %copy.22, bf16[256,1024]{1,0:T(8,128)(2,1)} %copy-done.3, bf16[256,256]{1,0:T(8,128)(2,1)S(1)} %copy-done.10, f32[]{:T(128)} %bitcast), kind=kOutput, calls=%fused_computation.18 | convolution fusion | flops 134742016 | bytes 3801092 | tf_op jit(solution)/shard_map/dot_general | solution.py:317
  119.3 1.3 %copy.24 = f32[256,1024]{1,0:T(8,128)} copy(f32[256,1024]{0,1:T(8,128)S(1)} %get-tuple-element.39) | data formatting | bytes 2097152
  120.6 1.3 %copy.25 = f32[256,1024]{1,0:T(8,128)} copy(f32[256,1024]{0,1:T(8,128)S(1)} %get-tuple-element.38) | data formatting | bytes 2097152
  (13 shorter events, 0.1 us)
Async XLA Ops:
  0.6 3.8 %copy-start.9 = (f32[128,512]{1,0:T(8,128)S(1)}, f32[128,512]{1,0:T(8,128)}, u32[]{:S(2)}) copy-start(f32[128,512]{1,0:T(8,128)} %param.17) | copy-start | bytes 786436
  5.1 98.0 %copy-start.4 = (f32[256,512]{1,0:T(8,128)S(1)}, f32[256,512]{1,0:T(8,128)}, u32[]{:S(2)}) copy-start(f32[256,512]{1,0:T(8,128)} %mean_v.1) | copy-start | bytes 1572868
  5.1 98.0 %copy-start.5 = (f32[256,512]{1,0:T(8,128)S(1)}, f32[256,512]{1,0:T(8,128)}, u32[]{:S(2)}) copy-start(f32[256,512]{1,0:T(8,128)} %sq_v.1) | copy-start | bytes 1572868
  103.1 4.5 %copy-start.6 = (bf16[8,384,256]{2,1,0:T(8,128)(2,1)S(1)}, bf16[8,384,256]{2,1,0:T(8,128)(2,1)}, u32[]{:S(2)}) copy-start(bf16[8,384,256]{2,1,0:T(8,128)(2,1)} %get-tuple-element.18) | copy-start | bytes 4718596
  103.1 4.5 %copy-start.8 = (bf16[8,128,512]{2,1,0:T(8,128)(2,1)S(1)}, bf16[8,128,512]{2,1,0:T(8,128)(2,1)}, u32[]{:S(2)}) copy-start(bf16[8,128,512]{2,1,0:T(8,128)(2,1)} %get-tuple-element.19) | copy-start | bytes 3145732
  105.5 3.5 %copy-start.1 = (f32[256,1024]{1,0:T(8,128)S(1)}, f32[256,1024]{1,0:T(8,128)}, u32[]{:S(2)}) copy-start(f32[256,1024]{1,0:T(8,128)} %mean_o.1) | copy-start | bytes 3145732
  105.5 3.5 %copy-start.2 = (f32[256,1024]{1,0:T(8,128)S(1)}, f32[256,1024]{1,0:T(8,128)}, u32[]{:S(2)}) copy-start(f32[256,1024]{1,0:T(8,128)} %sq_o.1) | copy-start | bytes 3145732
  105.5 3.5 %copy-start.7 = (f32[256,1536]{1,0:T(8,128)S(1)}, f32[256,1536]{1,0:T(8,128)}, u32[]{:S(2)}) copy-start(f32[256,1536]{1,0:T(8,128)} %get-tuple-element.16) | copy-start | bytes 4718596
  109.0 3.1 %copy-start.12 = (bf16[8,256,1024]{2,1,0:T(8,128)(2,1)S(1)}, bf16[8,256,1024]{2,1,0:T(8,128)(2,1)}, u32[]{:S(2)}) copy-start(bf16[8,256,1024]{2,1,0:T(8,128)(2,1)} %get-tuple-element.17) | copy-start | bytes 12582916
  110.7 1.3 %copy-start.3 = (bf16[256,1024]{1,0:T(8,128)(2,1)}, bf16[256,1024]{1,0:T(8,128)(2,1)S(1)}, u32[]{:S(2)}) copy-start(bf16[256,1024]{1,0:T(8,128)(2,1)S(1)} %get-tuple-element.33) | copy-start | bytes 1572868
  112.1 3.4 %copy-start.11 = (bf16[128,256]{1,0:T(8,128)(2,1)S(1)}, bf16[128,256]{1,0:T(8,128)(2,1)}, u32[]{:S(2)}) copy-start(bf16[128,256]{1,0:T(8,128)(2,1)} %param.19) | copy-start | bytes 196612
  115.4 2.1 %copy-start = (f32[256,1024]{1,0:T(8,128)S(1)}, f32[256,1024]{1,0:T(8,128)}, u32[]{:S(2)}) copy-start(f32[256,1024]{1,0:T(8,128)} %param.16) | copy-start | bytes 3145732
  115.6 2.3 %copy-start.10 = (bf16[256,256]{1,0:T(8,128)(2,1)S(1)}, bf16[256,256]{1,0:T(8,128)(2,1)}, u32[]{:S(2)}) copy-start(bf16[256,256]{1,0:T(8,128)(2,1)} %param.18) | copy-start | bytes 393220

commit v2 on v1

v2 whole, which is shorter than its diff:
```python
import functools

import jax
import jax.numpy as jnp
from jax import lax
from jax.experimental import pallas as pl
from jax.experimental.pallas import tpu as pltpu
from jax.sharding import PartitionSpec as P

LEARN_RATE = 0.01
MEAN_DECAY = 0.8
BETA_SQUARE = 0.9
EPS_RMS = 1e-06
MESH = pl.DeviceIdType.MESH
F32, BF16 = jnp.float32, jnp.bfloat16


def moments(proj, mean_in, square_in):
    mean_new = MEAN_DECAY * mean_in + (1.0 - MEAN_DECAY) * proj
    square_new = BETA_SQUARE * square_in + (1.0 - BETA_SQUARE) * proj * proj
    return (mean_new, square_new, mean_new / jnp.sqrt(square_new))


def rcopy(src, dst, send, recv, fs, tp):
    return pltpu.make_async_remote_copy(
        src_ref=src, dst_ref=dst, send_sem=send, recv_sem=recv,
        device_id=(fs, tp), device_id_type=MESH,
    )


class LineGather:
    def __init__(self, own, buf, up, dn, d2, rz, rd, nz, f, t):
        self.own, self.buf, self.nz, self.t, self.f = own, buf, nz, t, f
        self.up, self.dn, self.d2, self.rz, self.rd = up, dn, d2, rz, rd
        self.z, self.c = lax.div(f, 2), lax.rem(f, 2)
        self.partner = f + 1 - 2 * self.c

    def copy(self, kind, zb, src=None):
        block = self.buf.at[zb * 2 + self.c]
        src = block if src is None else src
        if kind == "up":
            return rcopy(src, block, self.up.at[zb], self.rz.at[zb], self.f + 2, self.t)
        if kind == "dn":
            return rcopy(src, block, self.dn.at[zb], self.rz.at[zb], self.f - 2, self.t)
        return rcopy(src, block, self.d2.at[zb], self.rd.at[zb], self.partner, self.t)

    def spread(self, zb, src, up, dn):
        if up:
            @pl.when(self.z < self.nz - 1)
            def _():
                self.copy("up", zb, src).start()
        if dn:
            @pl.when(self.z > 0)
            def _():
                self.copy("dn", zb, src).start()
        self.copy("d2", zb, src).start()

    def begin(self):
        self.spread(self.z, self.own, True, True)

    def step(self, s):
        @pl.when(self.z >= s)
        def _():
            zb = self.z - s
            rcopy(self.buf.at[zb * 2 + self.c], self.buf.at[zb * 2 + self.c], self.up.at[zb],
                  self.rz.at[zb], self.partner, self.t).wait_recv()
            self.spread(zb, None, True, False)

        @pl.when(self.z + s <= self.nz - 1)
        def _():
            zb = self.z + s
            rcopy(self.buf.at[zb * 2 + self.c], self.buf.at[zb * 2 + self.c], self.dn.at[zb],
                  self.rz.at[zb], self.partner, self.t).wait_recv()
            self.spread(zb, None, False, True)

    def arrive(self):
        for zb in range(self.nz):
            block = self.buf.at[zb * 2 + 1 - self.c]
            rcopy(block, block, self.d2.at[zb], self.rd.at[zb], self.partner, self.t).wait_recv()

    def finish(self):
        for zb in range(self.nz):
            self.copy("d2", zb).wait_send()

            @pl.when((self.z >= zb) & (self.z < self.nz - 1))
            def _():
                self.copy("up", zb).wait_send()

            @pl.when((self.z <= zb) & (self.z > 0))
            def _():
                self.copy("dn", zb).wait_send()


def exchange(nf, nt, *refs):
    hbm_in, (b_o, b_v), rest = refs[:10], refs[10:12], refs[12:]
    wg, bg_out, tot_out, dirs_out = (rest[2 * k:2 * k + 2] for k in range(4))
    totals, rest = rest[8], rest[9:]
    held, rest = rest[:10], rest[10:]
    w16, bg, lift, rsb, lifted, part, psend, pbuf, zsend, zbuf, tot, dirs = (
        rest[2 * k:2 * k + 2] for k in range(12))
    (tsend, tbuf, isem, osem, lsem, bsem, wsem, rs_s, rs_r, ag_s, ag_r, p_s, p_r, z_s, z_r,
     g_s, g_r, gd_s, gd_r, t_s, t_r) = rest[24:]
    lefts, rights, weights, means, squares_in = (held[2 * k:2 * k + 2] for k in range(5))
    pair_of = (0, 1)

    nz = nf // 2
    f, t = lax.axis_index("fs"), lax.axis_index("tp")
    z, c = lax.div(f, 2), lax.rem(f, 2)
    partner = f + 1 - 2 * c
    rank = b_o.shape[1]
    tc, seg, per = lefts[0].shape[0] // nt, rank // nf, nf // nt
    peers_t = [lax.rem(t + s, nt) for s in range(1, nt)]
    peers_z = [lax.rem(z + s, nz) for s in range(1, nz)]

    fetch = [pltpu.make_async_copy(hbm_in[k], held[k], isem.at[k]) for k in range(10)]
    for one in fetch:
        one.start()

    barrier = pltpu.get_barrier_semaphore()
    pl.semaphore_signal(barrier, inc=1, device_id=(partner, t), device_id_type=MESH)
    for pz in peers_z:
        pl.semaphore_signal(barrier, inc=1, device_id=(pz * 2 + c, t), device_id_type=MESH)
    for pt in peers_t:
        pl.semaphore_signal(barrier, inc=1, device_id=(f, pt), device_id_type=MESH)
    pl.semaphore_wait(barrier, 1 + len(peers_z) + len(peers_t))

    gb = [LineGather(own, bg[i], *[bsem.at[i, k] for k in range(5)], nz, f, t)
          for i, own in enumerate((b_o, b_v))]
    gw = [LineGather(w16[i], wg[i], *[wsem.at[i, k] for k in range(5)], nz, f, t) for i in pair_of]
    for g in gb:
        g.begin()
    for i, own in enumerate((b_o, b_v)):
        bg[i][f] = own[...]
        fetch[4 + i].wait()
        w16[i][...] = weights[i][...].astype(BF16)
    for s in range(1, nz):
        for g in gb:
            g.step(s)
    mine = [pltpu.make_async_copy(w16[i], wg[i].at[f], lsem.at[i]) for i in pair_of]
    for i in pair_of:
        gw[i].begin()
        mine[i].start()

    for i in pair_of:
        gb[i].arrive()
        fetch[i].wait()
        rows = bg[i][pl.ds(t * per, per)]
        factor = rows.reshape(rows.shape[0] * rows.shape[1], rank)
        waiting = None
        for pt in peers_t + [t]:
            at = pl.ds(pl.multiple_of(pt * tc, tc), tc)
            lift[i][pt] = jnp.dot(lefts[i][at, :], factor, preferred_element_type=F32).astype(BF16)
            if waiting is not None:
                waiting.start()
            waiting = None
            if pt is not t:
                waiting = rcopy(lift[i].at[pt], rsb[i].at[t], rs_s.at[i, pt], rs_r.at[i, t], f, pt)

    third = (nz - 1 + 2) // 3
    steps = list(range(1, nz))

    def weights_on(some):
        for s in some:
            for g in gw:
                g.step(s)

    def contract(i, pt, first):
        at = pl.ds(pl.multiple_of(pt * tc, tc), tc)
        got = lax.dot_general(lifted[i][pt], rights[i][at, :], (((0,), (0,)), ((), ())),
                              preferred_element_type=F32)
        if first:
            part[i][...] = got
        else:
            part[i][...] += got

    def sum_tokens(i):
        total = lift[i][t].astype(F32)
        for pt in peers_t:
            rcopy(lift[i].at[pt], rsb[i].at[pt], rs_s.at[i, pt], rs_r.at[i, pt], f, pt).wait_recv()
            total = total + rsb[i][pt].astype(F32)
        lifted[i][t] = total.astype(BF16)
        for pt in peers_t:
            rcopy(lifted[i].at[t], lifted[i].at[t], ag_s.at[i, pt], ag_r.at[i, t], f, pt).start()
        fetch[2 + i].wait()
        contract(i, t, True)

    def piece(i, core, zz):
        return part[i][pl.ds(pl.multiple_of((core * nz + zz) * seg, seg), seg), :]

    pairs = [rcopy(psend[i], pbuf[i], p_s.at[i], p_r.at[i], partner, t) for i in pair_of]

    def line_send(i):
        for pt in peers_t:
            rcopy(lifted[i].at[pt], lifted[i].at[pt], ag_s.at[i, pt], ag_r.at[i, pt], f, pt).wait_recv()
            contract(i, pt, False)
        for zz in range(nz):
            psend[i][zz] = piece(i, 1 - c, zz).astype(BF16)
        pairs[i].start()
        pairs[i].wait_recv()
        for pz in peers_z:
            zsend[i][pz] = (piece(i, c, pz) + pbuf[i][pz].astype(F32)).astype(BF16)
        for pz in peers_z:
            rcopy(zsend[i].at[pz], zbuf[i].at[z], z_s.at[i, pz], z_r.at[i, z], pz * 2 + c, t).start()

    me = c * nz + z

    def line_sum(i):
        acc = piece(i, c, z) + pbuf[i][z].astype(F32)
        for pz in peers_z:
            rcopy(zsend[i].at[pz], zbuf[i].at[pz], z_s.at[i, pz], z_r.at[i, pz], pz * 2 + c, t).wait_recv()
            acc = acc + zbuf[i][pz].astype(F32)
        tot[i][me] = acc.astype(BF16)
        own = tot[i].at[me]
        for pz in peers_z:
            rcopy(own, own, g_s.at[i, pz], g_r.at[i, z], pz * 2 + c, t).start()
        rcopy(own, own, gd_s.at[i, z], gd_r.at[i, z], partner, t).start()

    def line_take(i):
        for pz in peers_z:
            got = tot[i].at[c * nz + pz]
            rcopy(got, got, g_s.at[i, pz], g_r.at[i, pz], pz * 2 + c, t).wait_recv()
            rcopy(got, got, gd_s.at[i, pz], gd_r.at[i, pz], partner, t).start()
        for zz in range(nz):
            got = tot[i].at[(1 - c) * nz + zz]
            rcopy(got, got, gd_s.at[i, zz], gd_r.at[i, zz], partner, t).wait_recv()

    outs = [[pltpu.make_async_copy(src[i], dst[i], osem.at[k, i])
             for i in pair_of] for k, (src, dst) in enumerate(((bg, bg_out), (tot, tot_out), (dirs, dirs_out)))]

    def direct(i):
        fetch[6 + i].wait()
        fetch[8 + i].wait()
        part[i][...] = tot[i][...].astype(F32).reshape(part[i].shape)
        dirs[i][...] = moments(part[i][...], means[i][...], squares_in[i][...])[2].astype(BF16)

        def squares(g, sums):
            u = jnp.dot(bg[i][g], dirs[i][...], preferred_element_type=F32)
            return sums + jnp.sum(u * u, axis=0, keepdims=True)

        sums = lax.fori_loop(0, nf, squares, jnp.zeros((1, part[i].shape[1]), F32))
        tile = jnp.zeros((8, 128), F32) + jnp.sum(sums, axis=1, keepdims=True)
        tsend[i] = tile
        tbuf[t, i] = tile

    for i in pair_of:
        outs[0][i].start()
    weights_on(steps[:third])
    for i in pair_of:
        sum_tokens(i)
    weights_on(steps[third:2 * third])
    for i in pair_of:
        line_send(i)
    for i in pair_of:
        line_sum(i)
    weights_on(steps[2 * third:])
    for i in pair_of:
        line_take(i)
        direct(i)
    for pt in peers_t:
        rcopy(tsend, tbuf.at[t], t_s.at[pt], t_r.at[t], f, pt).start()
    for k in (1, 2):
        for i in pair_of:
            outs[k][i].start()
    for i in pair_of:
        mine[i].wait()
        gw[i].arrive()
        gb[i].finish()
        gw[i].finish()
        pairs[i].wait_send()
        for pt in peers_t:
            rcopy(lift[i].at[pt], rsb[i].at[t], rs_s.at[i, pt], rs_r.at[i, t], f, pt).wait_send()
            rcopy(lifted[i].at[t], lifted[i].at[t], ag_s.at[i, pt], ag_r.at[i, t], f, pt).wait_send()
        for pz in peers_z:
            rcopy(zsend[i].at[pz], zbuf[i].at[z], z_s.at[i, pz], z_r.at[i, z], pz * 2 + c, t).wait_send()
            own = tot[i].at[me]
            rcopy(own, own, g_s.at[i, pz], g_r.at[i, z], pz * 2 + c, t).wait_send()
        for zz in range(nz):
            got = tot[i].at[c * nz + zz]
            rcopy(got, got, gd_s.at[i, zz], gd_r.at[i, zz], partner, t).wait_send()
        for k in range(3):
            outs[k][i].wait()
    for pt in peers_t:
        rcopy(tsend, tbuf.at[pt], t_s.at[pt], t_r.at[pt], f, pt).wait_recv()
    summed = tbuf[0]
    for k in range(1, nt):
        summed = summed + tbuf[k]
    totals[...] = summed
    for pt in peers_t:
        rcopy(tsend, tbuf.at[t], t_s.at[pt], t_r.at[t], f, pt).wait_send()


def gather_and_reduce(nf, nt, lefts, rights, weights, bases, means, squares):
    rank, nz, tokens = bases[0].shape[1], nf // 2, rights[0].shape[0]
    tc, seg = tokens // nt, rank // nf
    heights, widths = [b.shape[0] for b in bases], [r.shape[1] for r in rights]
    vmem, dma = pl.BlockSpec(memory_space=pltpu.VMEM), pltpu.SemaphoreType.DMA
    hbm = pl.BlockSpec(memory_space=pltpu.HBM)
    fetched = (*lefts, *rights, *weights, *means, *squares)

    def two(shape_of, kind=BF16, make=pltpu.VMEM):
        return [make(shape_of(h, w), kind) for h, w in zip(heights, widths)]

    def outs(shape_of):
        return two(shape_of, make=jax.ShapeDtypeStruct)

    token_chunks = lambda h, w: (nt, tc, rank)
    line_pieces = lambda h, w: (nz, seg, w)
    return pl.pallas_call(
        functools.partial(exchange, nf, nt),
        out_shape=(
            *outs(lambda h, w: (nf, h, w)), *outs(lambda h, w: (nf, h, rank)),
            *outs(lambda h, w: (nf, seg, w)), *outs(lambda h, w: (rank, w)),
            jax.ShapeDtypeStruct((2, 8, 128), F32),
        ),
        in_specs=[hbm] * 10 + [vmem] * 2,
        out_specs=(hbm,) * 8 + (vmem,),
        scratch_shapes=[
            *[pltpu.VMEM(x.shape, x.dtype) for x in fetched],
            *two(lambda h, w: (h, w)), *two(lambda h, w: (nf, h, rank)),
            *two(token_chunks), *two(token_chunks), *two(token_chunks),
            *two(lambda h, w: (rank, w), F32),
            *two(line_pieces), *two(line_pieces), *two(line_pieces), *two(line_pieces),
            *two(lambda h, w: (nf, seg, w)), *two(lambda h, w: (rank, w)),
            pltpu.VMEM((2, 8, 128), F32),
            pltpu.VMEM((nt, 2, 8, 128), F32),
            dma((10,)), dma((3, 2)), dma((2,)), dma((2, 5, nz)), dma((2, 5, nz)),
            dma((2, nt)), dma((2, nt)), dma((2, nt)), dma((2, nt)), dma((2,)), dma((2,)),
            dma((2, nz)), dma((2, nz)), dma((2, nz)), dma((2, nz)), dma((2, nz)), dma((2, nz)),
            dma((nt,)), dma((nt,)),
        ],
        compiler_params=pltpu.CompilerParams(
            collective_id=0, has_side_effects=True, vmem_limit_bytes=56 * 1024 * 1024
        ),
        name="exchange",
    )(*fetched, *bases)


def apply(nt, *refs):
    parts, totals = [refs[8 * i:8 * i + 8] for i in range(2)], refs[16]
    outs = [refs[17 + 5 * i:22 + 5 * i] for i in range(2)]
    g, steps = pl.program_id(0), pl.num_programs(0)
    for i in range(2):
        proj, mean_in, square_in, direction, gathered, factor, basis, weight = parts[i]
        step, new, copy, mean, square = outs[i]
        count = gathered.shape[1] * steps * gathered.shape[2] * nt
        scale = LEARN_RATE * lax.rsqrt(totals[i, 0:1, 0:1] / lax.convert_element_type(count, F32) + EPS_RMS)
        p = proj[0].astype(F32)
        mean[...] = MEAN_DECAY * mean_in[...] + (1.0 - MEAN_DECAY) * p
        square[...] = BETA_SQUARE * square_in[...] + (1.0 - BETA_SQUARE) * p * p
        update = jnp.dot(factor[0], direction[...], preferred_element_type=F32)
        copy[...] = (gathered[0].astype(F32) - scale * update).astype(BF16)

        @pl.when(g == 0)
        def _():
            own = scale * jnp.dot(basis[...], direction[...], preferred_element_type=F32)
            step[...] = own
            new[...] = weight[...] - own


def finish(nf, nt, args, totals):
    whole = lambda x: pl.BlockSpec(x.shape, lambda g: (0,) * x.ndim)
    third = lambda x: pl.BlockSpec((1,) + x.shape[1:], lambda g: (g, 0, 0))
    rows = lambda x: pl.BlockSpec((x.shape[0] // nf, x.shape[1]), lambda g: (g, 0))
    in_specs, out_specs, out_shape = [], [], []
    for proj, mean_in, square_in, direction, gathered, factor, basis, weight in args:
        in_specs += [third(proj), rows(mean_in), rows(square_in), whole(direction), third(gathered),
                     third(factor), whole(basis), whole(weight)]
        copy = jax.ShapeDtypeStruct((nf * weight.shape[0], weight.shape[1]), BF16)
        like = lambda x: jax.ShapeDtypeStruct(x.shape, F32)
        out_shape += [like(weight), like(weight), copy, like(mean_in), like(square_in)]
        out_specs += [whole(weight), whole(weight), rows(copy), rows(mean_in), rows(square_in)]
    return pl.pallas_call(
        functools.partial(apply, nt),
        grid=(nf,),
        in_specs=in_specs + [whole(totals)],
        out_specs=out_specs,
        out_shape=out_shape,
        compiler_params=pltpu.CompilerParams(dimension_semantics=("arbitrary",)),
        name="apply",
    )(*args[0], *args[1], totals)


def per_device(nf, nt, attn_out, out_cot, latent, value_cot, out_weight, value_up_matrix,
               out_basis, value_basis, out_mean, out_square, value_mean, value_square):
    wg_o, wg_v, bg_o, bg_v, tot_o, tot_v, dirs_o, dirs_v, totals = gather_and_reduce(
        nf, nt, (attn_out, latent), (out_cot, value_cot), (out_weight, value_up_matrix),
        (out_basis, value_basis), (out_mean, value_mean), (out_square, value_square))
    return tuple(finish(nf, nt, (
        (tot_o, out_mean, out_square, dirs_o, wg_o, bg_o, out_basis, out_weight),
        (tot_v, value_mean, value_square, dirs_v, wg_v, bg_v, value_basis, value_up_matrix),
    ), totals))


def solution(mesh):
    both, rows, cols = P("fs", "tp"), P("fs", None), P(None, "tp")
    return jax.shard_map(
        functools.partial(per_device, mesh.shape["fs"], mesh.shape["tp"]),
        mesh=mesh,
        in_specs=(both,) * 6 + (rows,) * 2 + (cols,) * 4,
        out_specs=(both, both, cols, cols, cols) * 2,
        check_vma=False,
    )
```

time: 122 us -> 103 us (0.84)
  other arithmetic: 8.53 us -> 0 us
  local copies, waits for them, and re-layouts: 6.39 us -> 0 us
  matrix products: 6.36 us -> 0 us
  Pallas kernels: 97.9 us -> 102 us
  between operations: 2.68 us -> 0.65 us
    convert_element_type x4 -> x0, other arithmetic: 6.89 us -> none  [the longest x2 4.08 us: finish(): narrow = direction.astype(BF16)]
    dot_general x4 -> x0, matrix products: 6.36 us -> none  [the longest x2 4.68 us: finish(): every = jnp.dot(whole.reshape(rows, -1), narrow, preferred_element_type=F32)]
    unnamed x32 -> x0, local copies, waits for them, and re-layouts: 4.93 us -> none
    pallas_call x1 -> x2, Pallas kernels: 97.9 us -> 102 us  [the longest x1 88.9 us: gather_and_reduce(): pl.pallas_call(functools.partial(exchange, nf, nt), out_shape=(*outs(lamb...]
    concatenate x1 -> x0, other arithmetic: 1.63 us -> none  [gather_and_reduce(): basis = jnp.concatenate((b_o, b_v), axis=0)]
    slice x3 -> x0, local copies, waits for them, and re-layouts: 1.45 us -> none  [the longest x1 1.35 us: per_device(): totals[1, 0, 0]]
where the time goes in v2:
time: 103 us
  Pallas kernels  102 us (99%)
    pallas_call x1, Pallas kernels, gather_and_reduce(): pl.pallas_call(functools.partial(exchange, nf, nt), out_shape=(*outs(lamb...  88.9 us
    pallas_call x1, Pallas kernels, finish(): pl.pallas_call(functools.partial(apply, nt), grid=(nf,), in_specs=in_spec...  13.5 us

profile of v2, /device:TPU:0, one launch (start us, length us, event | category | flops | bytes accessed | tf_op | source)
XLA Modules:
  0.0 103.1 jit_solution(10514559008447595337)
XLA Ops:
  0.6 88.9 %exchange.1 = (bf16[8,256,1024]{2,1,0:T(8,128)(2,1)}, bf16[8,128,512]{2,1,0:T(8,128)(2,1)}, bf16[8,256,256]{2,1,0:T(8,128)(2,1)}, bf16[8,128,256]{2,1,0:T(8,128)...) custom-call(bf16[1536,512]{1,0:T(8,128)(2,1)} %refs_0_.1, ...), custom_call_target="tpu_custom_call" | custom-call | tf_op jit(solution)/shard_map/exchange/pallas_call | solution.py:308
  89.6 13.5 %apply.1 = (f32[256,1024]{1,0:T(8,128)}, f32[256,1024]{1,0:T(8,128)}, bf16[2048,1024]{1,0:T(8,128)(2,1)}, f32[256,1024]{1,0:T(8,128)}, f32[256,1024]{1,0:T(8,128...) custom-call(bf16[8,32,1024]{2,1,0:T(8,128)(2,1)} %get-tuple-element., ...), custom_call_target="tpu_custom_call" | custom-call | tf_op jit(solution)/shard_map/apply/pallas_call | solution.py:372
